TPU v7x, 32 devices: a whole 2x2x4 slice. The times are simulated.
32 devices in a mesh: fs: 16 (over z, y, x), tp: 2 (over core).
Axes of the slice: x: 2, y: 2, z: 4, core: 2. Of those that a mesh axis runs over, the one named last changes fastest.
Arguments:
- tokens: bfloat16 [3072, 2048], P('fs'), may hold values from -6 to 6
- route_ids: int32 [3072, 2], P('fs'), may hold values from 0 to 7, all different within a row; in each aligned block of 192 rows (0 to 191, 192 to 383, ...) at most 96 rows name the same one
- route_logits: float32 [3072, 2], P('fs'), may hold values from -6 to 6
- norm_gain: float32 [2048], P('fs'), may hold values from 0.1 to 1.9
- gate_weight: float32 [8, 2048, 2048], P(None, 'fs', 'tp'), may hold values from -0.125 to 0.125
- up_weight: float32 [8, 2048, 2048], P(None, 'fs', 'tp'), may hold values from -0.125 to 0.125
- down_weight: float32 [8, 2048, 2048], P(None, 'fs', 'tp'), may hold values from -0.125 to 0.125
Outputs:
- mixed: bfloat16 [3072, 2048], P('fs')
- gate_copies: bfloat16 [16, 2048, 2048], P('fs', None, 'tp')
- up_copies: bfloat16 [16, 2048, 2048], P('fs', None, 'tp')
- down_copies: bfloat16 [16, 2048, 2048], P('fs', None, 'tp')
Inputs may be any that keep to these rules, and one draw needn't show every extreme that they name: `route_ids`: each row names 2 different experts. Among the rows of one index of fs no expert is named by more than 96 rows, a bound that some of them reach.
All inputs are finite; a program needn't handle non-finite values.
Results may differ from a plain program's by a relative error of at most 0.014.
Values may be sent and summed in bfloat16 or wider, within the bound.
A program may use at most 128 MiB of HBM per device.

v0:
```python
import jax
import jax.numpy as jnp
from jax import lax
from jax.sharding import PartitionSpec as P

CAP = 96


def body(tokens, route_ids, route_logits, norm_gain, gate_weight, up_weight, down_weight):
    experts = gate_weight.shape[0]
    fs_count = lax.axis_size("fs")
    copies = fs_count // experts
    per_peer = CAP // copies
    tok_rows = tokens.shape[0]
    width = tokens.shape[1]
    scaled_gain = norm_gain[None, :, None]
    gate_send = jnp.repeat((scaled_gain * gate_weight).astype(jnp.bfloat16), copies, axis=0)
    up_send = jnp.repeat((scaled_gain * up_weight).astype(jnp.bfloat16), copies, axis=0)
    down_send = jnp.repeat(down_weight.astype(jnp.bfloat16), copies, axis=0)
    gate_new, up_new, down_new = (
        lax.all_to_all(gate_send, "fs", split_axis=0, concat_axis=1, tiled=True),
        lax.all_to_all(up_send, "fs", split_axis=0, concat_axis=1, tiled=True),
        lax.all_to_all(down_send, "fs", split_axis=0, concat_axis=1, tiled=True),
    )
    values = tokens.astype(jnp.float32)
    center = jnp.mean(values, axis=1, keepdims=True)
    spread = jnp.mean(jnp.square(values - center), axis=1, keepdims=True)
    normed = ((values - center) * lax.rsqrt(spread + 1e-06)).astype(jnp.bfloat16)
    flat_ids = route_ids.reshape(-1)
    onehot_table = (flat_ids[:, None] == jnp.arange(experts, dtype=jnp.int32)[None, :]).astype(
        jnp.int32
    )
    before = jnp.cumsum(onehot_table, axis=0) - onehot_table
    order_rank = jnp.sum(before * onehot_table, axis=1)
    dest_flat = (flat_ids * copies + order_rank % copies) * per_peer + order_rank // copies
    owners = jnp.arange(flat_ids.shape[0], dtype=jnp.int32) // route_ids.shape[1]
    slot_token = jnp.full((experts * CAP,), tok_rows, jnp.int32).at[dest_flat].set(owners)
    padded = jnp.concatenate([normed, jnp.zeros((1, width), jnp.bfloat16)], axis=0)
    send_rows = padded[slot_token].reshape(fs_count, per_peer, width)
    gate_matrix = gate_new[0]
    up_matrix = up_new[0]
    col_count = width // lax.axis_size("tp")
    col_start = lax.axis_index("tp") * col_count
    own_cols = lax.dynamic_slice_in_dim(send_rows, col_start, col_count, 2)
    arrived = lax.all_to_all(own_cols, "fs", split_axis=0, concat_axis=0, tiled=True).reshape(
        -1, col_count
    )
    piece = lax.all_gather(arrived, "tp", axis=1, tiled=True)
    gate_act = jnp.dot(piece, gate_matrix, preferred_element_type=jnp.float32)
    up_act = jnp.dot(piece, up_matrix, preferred_element_type=jnp.float32)
    hidden = (jax.nn.silu(gate_act) * up_act).astype(jnp.bfloat16)
    partial_value = jnp.einsum("rf,df->rd", hidden, down_new[0], preferred_element_type=jnp.float32)
    share = lax.psum_scatter(
        partial_value.astype(jnp.bfloat16), "tp", scatter_dimension=1, tiled=True
    )
    back_part = lax.all_to_all(
        share.reshape(fs_count, per_peer, col_count), "fs", split_axis=0, concat_axis=0, tiled=True
    )
    returned = lax.all_gather(back_part, "tp", axis=2, tiled=True).reshape(-1, width)
    picked = returned[dest_flat].reshape(tok_rows, route_ids.shape[1], width).astype(jnp.float32)
    first_weight = jax.nn.sigmoid(route_logits[:, 0] - route_logits[:, 1])
    second_weight = jax.nn.sigmoid(route_logits[:, 1] - route_logits[:, 0])
    mixed = (first_weight[:, None] * picked[:, 0] + second_weight[:, None] * picked[:, 1]).astype(
        jnp.bfloat16
    )
    return (mixed, gate_new, up_new, down_new)


def solution(mesh):
    return jax.shard_map(
        body,
        mesh=mesh,
        in_specs=(
            P("fs", None),
            P("fs", None),
            P("fs", None),
            P("fs"),
            P(None, "fs", "tp"),
            P(None, "fs", "tp"),
            P(None, "fs", "tp"),
        ),
        out_specs=(P("fs", None), P("fs", None, "tp"), P("fs", None, "tp"), P("fs", None, "tp")),
        check_vma=False,
    )
```

profile of v0, /device:TPU:0, one launch (start us, length us, event | category | flops | bytes accessed | tf_op | source)
XLA Modules:
  0.0 482.2 jit_solution(4758031760930865264)
XLA Ops:
  7.2 0.8 copy.14
  8.0 0.1 eq.31
  8.1 0.1 eq.27
  8.3 0.7 broadcast_multiply_fusion
  9.0 0.9 reduce-window.6
  9.8 0.2 slice_reduce_fusion
  10.1 0.1 copy.13
  10.2 0.1 mul.92
  10.4 0.1 fusion.9
  10.5 2.9 scatter_custom_fusion
  13.4 1.3 convert_reduce_fusion
  14.8 1.5 fusion.2
  16.3 1.6 fusion.3
  17.9 0.1 concatenate.3
  18.0 4.2 gather_fusion
  22.2 0.0 copy-start.2
  22.2 2.7 constant_dynamic-slice_fusion
  24.9 8.4 %all-to-all-start = ((bf16[16,48,1024]{2,1,0:T(8,128)(2,1)}), bf16[16,48,1024]{2,1,0:T(8,128)(2,1)}, u32[]{:S(2)}, u32[]{:S(2)}) async-start(bf16[16,48,1024]{2,1,0:T(8,128)(2,1)} %constant_dynamic-slice_fusion), calls=%async_computation | async-start | bytes 3145728 | tf_op jit(solution)/shard_map/all_to_all | solution.py:45
  33.3 0.0 copy-done.2
  33.3 6.1 %multiply_convert_fusion = (bf16[8,128,1024]{2,1,0:T(8,128)(2,1)S(1)}, bf16[8,128,1024]{2,1,0:T(8,128)(2,1)}) fusion(f32[8,128,1024]{2,1,0:T(8,128)} %param.12, f32[128]{0:T(128)S(1)} %copy-done.2, f32[8,128,1024]{2,1,0:T(8,128)} %param.11), kind=kLoop, calls=%fused_computation.3 | loop fusion | flops 4194304 | bytes 12583424 | tf_op jit(solution)/shard_map/convert_element_type | solution.py:18
  39.4 28.0 %all-to-all-done = bf16[16,48,1024]{2,1,0:T(8,128)(2,1)} async-done(((bf16[16,48,1024]{2,1,0:T(8,128)(2,1)}), bf16[16,48,1024]{2,1,0:T(8,128)(2,1)}, u32[]{:S(2)}, u32[]{:S(2)}) %all-to-all-start) | async-done | bytes 1572896 | tf_op jit(solution)/shard_map/all_to_all | solution.py:45
  67.5 2.1 broadcast_in_dim.12
  69.6 100.9 %all_to_all.46 = bf16[16,128,1024]{2,1,0:T(8,128)(2,1)} all-to-all(bf16[16,128,1024]{2,1,0:T(8,128)(2,1)S(1)} %bitcast.48), channel_id=1, replica_groups=mesh['fs'=16,'tp'=2] {'fs'}, dimensions={0} | all-to-all | bytes 8388608 | tf_op jit(solution)/shard_map/all_to_all | solution.py:21
  170.5 2.6 broadcast_in_dim.13
  173.1 4.5 all-to-all-start.2
  177.6 2.5 convert_element_type.44
  180.2 75.9 %all-to-all-done.2 = bf16[16,128,1024]{2,1,0:T(8,128)(2,1)} async-done(((bf16[16,128,1024]{2,1,0:T(8,128)(2,1)}), bf16[16,128,1024]{2,1,0:T(8,128)(2,1)}, u32[]{:S(2)}, u32[]{:S(2)}) %all-to-all-start.2) | async-done | bytes 4194336 | tf_op jit(solution)/shard_map/all_to_all | solution.py:22
  256.1 2.6 broadcast_in_dim.28
  258.7 18.6 %all-to-all-start.3 = ((bf16[16,128,1024]{2,1,0:T(8,128)(2,1)}), bf16[16,128,1024]{2,1,0:T(8,128)(2,1)}, u32[]{:S(2)}, u32[]{:S(2)}) async-start(bf16[16,128,1024]{2,1,0:T(8,128)(2,1)} %bitcast.46), calls=%async_computation.3 | async-start | bytes 8388608 | tf_op jit(solution)/shard_map/all_to_all | solution.py:23
  277.3 0.0 all-gather.3.cloned.1.call-start
  277.3 0.7 all-gather.3.cloned.1.call-update
  278.0 0.2 reduce-scatter.2.cloned.1.call-start
  278.2 14.8 %all-gather.3.cloned.1.call-done = bf16[768,2048]{1,0:T(8,128)(2,1)} async-done(((bf16[768,1024]{1,0:T(8,128)(2,1)}), bf16[768,2048]{1,0:T(8,128)(2,1)}) %all-gather.3.cloned.1.call-update) | async-done | bytes 3145744 | tf_op jit(solution)/shard_map/all_gather | solution.py:48
  293.0 8.2 %fusion.20 = f32[768,1024]{1,0:T(8,128)} fusion(bf16[768,2048]{1,0:T(8,128)(2,1)} %all-gather.3.cloned.1.call-done, bf16[2048,1024]{1,0:T(8,128)(2,1)} %bitcast.44), kind=kOutput, calls=%fused_computation.54 | convolution fusion | flops 3221225472 | bytes 10485760 | tf_op jit(solution)/shard_map/dot_general | solution.py:49
  301.2 54.5 %all-to-all-done.3 = bf16[16,128,1024]{2,1,0:T(8,128)(2,1)} async-done(((bf16[16,128,1024]{2,1,0:T(8,128)(2,1)}), bf16[16,128,1024]{2,1,0:T(8,128)(2,1)}, u32[]{:S(2)}, u32[]{:S(2)}) %all-to-all-start.3) | async-done | bytes 4194336 | tf_op jit(solution)/shard_map/all_to_all | solution.py:23
  355.7 12.5 %convolution_convert_fusion = bf16[768,2048]{1,0:T(8,128)(2,1)} fusion(bf16[2048,1024]{1,0:T(8,128)(2,1)} %bitcast.10, f32[768,1024]{1,0:T(8,128)} %fusion.20, bf16[768,2048]{1,0:T(8,128)(2,1)} %all-gather.3.cloned.1.call-done, bf16[2048,1024]{1,0:T(8,128)(2,1)} %bitcast.8), kind=kOutput, calls=%fused_computation.5 | convolution fusion | flops 6448742400 | bytes 17825792 | tf_op jit(solution)/shard_map/rf,df->rd/dot_general | solution.py:52
  368.3 0.0 reduce-scatter.2.cloned.1.call-update
  368.3 0.0 copy-start.1
  368.3 0.0 all-gather.5.cloned.1.call-start
  368.4 24.9 %reduce-scatter.2.cloned.1.call-done = bf16[768,1024]{1,0:T(8,128)(2,1)} async-done(((bf16[768,2048]{1,0:T(8,128)(2,1)}), bf16[768,1024]{1,0:T(8,128)(2,1)}) %reduce-scatter.2.cloned.1.call-update) | async-done | bytes 1572880 | tf_op jit(solution)/shard_map/reduce_scatter | solution.py:53
  393.2 44.9 %all_to_all.47 = bf16[16,48,1024]{2,1,0:T(8,128)(2,1)} all-to-all(bf16[16,48,1024]{2,1,0:T(8,128)(2,1)} %bitcast.50), channel_id=1, replica_groups=mesh['fs'=16,'tp'=2] {'fs'}, dimensions={0} | all-to-all | bytes 3145728 | tf_op jit(solution)/shard_map/all_to_all | solution.py:56
  438.1 0.0 all-gather.5.cloned.1.call-update
  438.1 0.0 copy-done.1
  438.2 10.6 %all-gather.5.cloned.1.call-done = bf16[16,48,2048]{2,1,0:T(8,128)(2,1)} async-done(((bf16[16,48,1024]{2,1,0:T(8,128)(2,1)}), bf16[16,48,2048]{2,1,0:T(8,128)(2,1)}) %all-gather.5.cloned.1.call-update) | async-done | bytes 3145744 | tf_op jit(solution)/shard_map/all_gather | solution.py:59
  448.7 7.3 %gather_fusion.1 = bf16[384,2048]{1,0:T(8,128)(2,1)} fusion(bf16[768,2048]{1,0:T(8,128)(2,1)} %bitcast.43, s32[1024]{0:T(1024)S(1)} %pad_clamp_fusion), kind=kCustom, calls=%fused_computation.1 | custom fusion | bytes 3147264 | tf_op jit(solution)/shard_map/gather | solution.py:60
  456.1 3.4 reshape.184
  459.5 0.0 copy-start
  459.5 2.4 fusion.19
  461.9 2.5 fusion.6
  464.4 0.0 copy-done
  464.4 2.0 copy.35
  466.4 4.6 copy.36
  471.0 4.6 copy.37
  (10 shorter events, 0.1 us)
Async XLA Ops:
  22.2 11.1 %copy-start.2 = (f32[128]{0:T(128)S(1)}, f32[128]{0:T(128)}, u32[]{:S(2)}) copy-start(f32[128]{0:T(128)} %param.10) | copy-start | bytes 1540
  24.9 42.6 %all-to-all-start = ((bf16[16,48,1024]{2,1,0:T(8,128)(2,1)}), bf16[16,48,1024]{2,1,0:T(8,128)(2,1)}, u32[]{:S(2)}, u32[]{:S(2)}) async-start(bf16[16,48,1024]{2,1,0:T(8,128)(2,1)} %constant_dynamic-slice_fusion), calls=%async_computation | async-start | bytes 3145728 | tf_op jit(solution)/shard_map/all_to_all | solution.py:45
  173.1 83.0 %all-to-all-start.2 = ((bf16[16,128,1024]{2,1,0:T(8,128)(2,1)}), bf16[16,128,1024]{2,1,0:T(8,128)(2,1)}, u32[]{:S(2)}, u32[]{:S(2)}) async-start(bf16[16,128,1024]{2,1,0:T(8,128)(2,1)} %bitcast.47), calls=%async_computation.2 | async-start | bytes 8388608 | tf_op jit(solution)/shard_map/all_to_all | solution.py:22
  258.7 97.0 %all-to-all-start.3 = ((bf16[16,128,1024]{2,1,0:T(8,128)(2,1)}), bf16[16,128,1024]{2,1,0:T(8,128)(2,1)}, u32[]{:S(2)}, u32[]{:S(2)}) async-start(bf16[16,128,1024]{2,1,0:T(8,128)(2,1)} %bitcast.46), calls=%async_computation.3 | async-start | bytes 8388608 | tf_op jit(solution)/shard_map/all_to_all | solution.py:23
  277.3 15.7 %all-gather.3.cloned.1.call-start = ((), (), s32[]{:S(2)}) async-start(), calls=%async_computation.6 | async-start | bytes 4718592 | tf_op jit(solution)/shard_map/all_gather | solution.py:48
  278.0 115.2 %reduce-scatter.2.cloned.1.call-start = ((), (), s32[]{:S(2)}) async-start(), calls=%async_computation.7 | async-start | bytes 4718592 | tf_op jit(solution)/shard_map/reduce_scatter | solution.py:53
  368.3 69.8 %copy-start.1 = (f32[192,2]{0,1:T(2,128)S(1)}, f32[192,2]{0,1:T(2,128)}, u32[]{:S(2)}) copy-start(f32[192,2]{0,1:T(2,128)} %param.9) | copy-start | bytes 4612
  368.3 80.4 %all-gather.5.cloned.1.call-start = ((), (), s32[]{:S(2)}) async-start(), calls=%async_computation.8 | async-start | bytes 4718592 | tf_op jit(solution)/shard_map/all_gather | solution.py:59
  459.5 4.9 %copy-start = (bf16[16,128,1024]{2,1,0:T(8,128)(2,1)S(1)}, bf16[16,128,1024]{2,1,0:T(8,128)(2,1)}, u32[]{:S(2)}) copy-start(bf16[16,128,1024]{2,1,0:T(8,128)(2,1)} %all_to_all.46) | copy-start | bytes 12582916
Sparse Core Ops, SparseCore 0:
  279.6 13.3 all-gather.2
  368.4 24.7 reduce-scatter.1
  438.2 10.4 all-gather.4
where the time goes:
time: 483 us; the launch traced here: 482 us
  waiting for transfers between devices  209 us (43%)
  blocking collectives  146 us (30%)
  local copies, waits for them, and re-layouts  43.4 us (9%)
  starting transfers between devices  31.8 us (7%)
  matrix products  20.8 us (4%)
  other arithmetic  17.3 us (4%)
  between operations  13.9 us (3%)
    all_to_all x1, blocking collectives, body(): lax.all_to_all(gate_send, 'fs', split_axis=0, concat_axis=1, tiled=True)  101 us
    all_to_all x1, waiting for transfers between devices, body(): lax.all_to_all(up_send, 'fs', split_axis=0, concat_axis=1, tiled=True)  75.9 us
    all_to_all x1, waiting for transfers between devices, body(): lax.all_to_all(down_send, 'fs', split_axis=0, concat_axis=1, tiled=True)  54.5 us
    all_to_all x1, blocking collectives, body(): lax.all_to_all(share.reshape(fs_count, per_peer, col_count), 'fs', split_...  44.9 us
    all_to_all x1, waiting for transfers between devices, body(): lax.all_to_all(own_cols, 'fs', split_axis=0, concat_axis=0, tiled=True)  28 us
    reduce_scatter x1, waiting for transfers between devices, body(): lax.psum_scatter(partial_value.astype(jnp.bfloat16), 'tp', scatter_dimens...  24.9 us
    all_to_all x1, starting transfers between devices, body(): lax.all_to_all(down_send, 'fs', split_axis=0, concat_axis=1, tiled=True)  18.6 us
    all_gather x1, waiting for transfers between devices, body(): piece = lax.all_gather(arrived, 'tp', axis=1, tiled=True)  14.8 us
  transfers between devices with their start and end apart: 6, of which 6 were waited for; matrix products, arithmetic and copies ran while one was open for 3% of the time, Pallas kernels for 0%

commit v1 on v0

--- a/solution.py
+++ b/solution.py
@@ -4,6 +4,12 @@
 from jax.sharding import PartitionSpec as P
 
 CAP = 96
+
+
+def swap_blocks(x, name, split, join):
+    shards = jnp.split(x, lax.axis_size(name), axis=split)
+    received = lax.all_to_all(jnp.stack(shards), name, 0, 0)
+    return jnp.concatenate(received, axis=join)
 
 
 def body(tokens, route_ids, route_logits, norm_gain, gate_weight, up_weight, down_weight):
@@ -19,7 +25,7 @@
     down_send = jnp.repeat(down_weight.astype(jnp.bfloat16), copies, axis=0)
     gate_new, up_new, down_new = (
         lax.all_to_all(gate_send, "fs", split_axis=0, concat_axis=1, tiled=True),
-        lax.all_to_all(up_send, "fs", split_axis=0, concat_axis=1, tiled=True),
+        swap_blocks(up_send, "fs", 0, 1),
         lax.all_to_all(down_send, "fs", split_axis=0, concat_axis=1, tiled=True),
     )
     values = tokens.astype(jnp.float32)

time: 483 us -> 481 us (level)
  local copies, waits for them, and re-layouts: 43.4 us -> 53.5 us
  waiting for transfers between devices: 209 us -> 199 us
    unnamed x10 -> x25, local copies, waits for them, and re-layouts: 12.1 us -> 23.1 us
    all_to_all x1, waiting for transfers between devices: 28 us -> 17.3 us  [body(): lax.all_to_all(own_cols, 'fs', split_axis=0, concat_axis=0, tiled=True)]
  transfers between devices with their start and end apart: 6 -> 6, of which waited for: 6 -> 6; matrix products, arithmetic and copies ran while one was open for 3% -> 6% of each run, Pallas kernels for 0% -> 0%
where the time goes in v1:
time: 481 us; the launch traced here: 480 us
  waiting for transfers between devices  199 us (41%)
  blocking collectives  146 us (30%)
  local copies, waits for them, and re-layouts  53.5 us (11%)
  starting transfers between devices  31.8 us (7%)
  matrix products  20.7 us (4%)
  other arithmetic  15.9 us (3%)
  between operations  13.9 us (3%)
    all_to_all x1, blocking collectives, swap_blocks(): received = lax.all_to_all(jnp.stack(shards), name, 0, 0)  101 us
    all_to_all x1, waiting for transfers between devices, body(): lax.all_to_all(gate_send, 'fs', split_axis=0, concat_axis=1, tiled=True)  75.9 us
    all_to_all x1, waiting for transfers between devices, body(): lax.all_to_all(down_send, 'fs', split_axis=0, concat_axis=1, tiled=True)  54.5 us
    all_to_all x1, blocking collectives, body(): lax.all_to_all(share.reshape(fs_count, per_peer, col_count), 'fs', split_...  44.9 us
    reduce_scatter x1, waiting for transfers between devices, body(): lax.psum_scatter(partial_value.astype(jnp.bfloat16), 'tp', scatter_dimens...  24.9 us
    unnamed x25, local copies, waits for them, and re-layouts  23.1 us
    all_to_all x1, starting transfers between devices, body(): lax.all_to_all(down_send, 'fs', split_axis=0, concat_axis=1, tiled=True)  18.5 us
    all_to_all x1, waiting for transfers between devices, body(): lax.all_to_all(own_cols, 'fs', split_axis=0, concat_axis=0, tiled=True)  17.3 us
  transfers between devices with their start and end apart: 6, of which 6 were waited for; matrix products, arithmetic and copies ran while one was open for 6% of the time, Pallas kernels for 0%

profile of v1, /device:TPU:0, one launch (start us, length us, event | category | flops | bytes accessed | tf_op | source)
XLA Modules:
  0.0 480.4 jit_solution(3566671061701294676)
XLA Ops:
  7.2 0.8 copy.49
  8.0 0.1 eq.31
  8.1 0.1 eq.27
  8.3 0.7 broadcast_multiply_fusion
  9.0 0.9 reduce-window.6
  9.8 0.2 slice_reduce_fusion
  10.1 0.1 copy.48
  10.2 0.1 mul.92
  10.4 0.1 fusion.25
  10.5 2.9 scatter_custom_fusion
  13.4 1.3 convert_reduce_fusion
  14.8 1.5 fusion.2
  16.3 1.6 fusion.3
  17.9 0.1 concatenate.3
  18.0 4.2 gather_fusion
  22.2 2.7 constant_dynamic-slice_fusion
  24.9 8.4 %all-to-all-start = ((bf16[16,48,1024]{2,1,0:T(8,128)(2,1)}), bf16[16,48,1024]{2,1,0:T(8,128)(2,1)}, u32[]{:S(2)}, u32[]{:S(2)}) async-start(bf16[16,48,1024]{2,1,0:T(8,128)(2,1)} %constant_dynamic-slice_fusion), calls=%async_computation | async-start | bytes 3145728 | tf_op jit(solution)/shard_map/all_to_all | solution.py:51
  33.3 0.0 copy-done.2
  33.3 4.8 multiply_convert_fusion
  38.1 0.5 broadcast_in_dim.13
  38.6 0.7 fusion.23
  39.4 0.7 fusion.22
  40.1 0.7 fusion.21
  40.8 0.7 fusion.20
  41.5 0.7 fusion.19
  42.3 0.7 fusion.18
  43.0 0.7 fusion.17
  43.7 0.7 fusion.16
  44.4 0.7 fusion.15
  45.1 0.7 fusion.14
  45.9 0.7 fusion.13
  46.6 0.7 fusion.12
  47.3 0.7 fusion.11
  48.0 0.7 fusion.10
  48.7 0.7 fusion.9
  49.5 0.7 fusion.8
  50.2 17.3 %all-to-all-done = bf16[16,48,1024]{2,1,0:T(8,128)(2,1)} async-done(((bf16[16,48,1024]{2,1,0:T(8,128)(2,1)}), bf16[16,48,1024]{2,1,0:T(8,128)(2,1)}, u32[]{:S(2)}, u32[]{:S(2)}) %all-to-all-start) | async-done | bytes 1572896 | tf_op jit(solution)/shard_map/all_to_all | solution.py:51
  67.5 101.1 %all_to_all.39 = bf16[16,1,128,1024]{3,2,1,0:T(8,128)(2,1)} all-to-all(bf16[16,1,128,1024]{3,2,1,0:T(8,128)(2,1)} %fusion.8), channel_id=1, replica_groups=mesh['fs'=16,'tp'=2] {'fs'}, dimensions={0} | all-to-all | bytes 8388608 | tf_op jit(solution)/shard_map/all_to_all | solution.py:11
  168.5 2.6 broadcast_in_dim.12
  171.2 4.6 all-to-all-start.1
  175.7 2.5 convert_element_type.44
  178.3 75.9 %all-to-all-done.1 = bf16[16,128,1024]{2,1,0:T(8,128)(2,1)} async-done(((bf16[16,128,1024]{2,1,0:T(8,128)(2,1)}), bf16[16,128,1024]{2,1,0:T(8,128)(2,1)}, u32[]{:S(2)}, u32[]{:S(2)}) %all-to-all-start.1) | async-done | bytes 4194336 | tf_op jit(solution)/shard_map/all_to_all | solution.py:27
  254.2 2.6 broadcast_in_dim.28
  256.8 18.5 %all-to-all-start.3 = ((bf16[16,128,1024]{2,1,0:T(8,128)(2,1)}), bf16[16,128,1024]{2,1,0:T(8,128)(2,1)}, u32[]{:S(2)}, u32[]{:S(2)}) async-start(bf16[16,128,1024]{2,1,0:T(8,128)(2,1)} %bitcast.126), calls=%async_computation.3 | async-start | bytes 8388608 | tf_op jit(solution)/shard_map/all_to_all | solution.py:29
  275.3 0.0 all-gather.3.cloned.1.call-start
  275.4 0.7 all-gather.3.cloned.1.call-update
  276.1 0.2 reduce-scatter.2.cloned.1.call-start
  276.3 14.8 %all-gather.3.cloned.1.call-done = bf16[768,2048]{1,0:T(8,128)(2,1)} async-done(((bf16[768,1024]{1,0:T(8,128)(2,1)}), bf16[768,2048]{1,0:T(8,128)(2,1)}) %all-gather.3.cloned.1.call-update) | async-done | bytes 3145744 | tf_op jit(solution)/shard_map/all_gather | solution.py:54
  291.1 8.2 %fusion.36 = f32[768,1024]{1,0:T(8,128)} fusion(bf16[768,2048]{1,0:T(8,128)(2,1)} %all-gather.3.cloned.1.call-done, bf16[2048,1024]{1,0:T(8,128)(2,1)} %bitcast.6), kind=kOutput, calls=%fused_computation.86 | convolution fusion | flops 3221225472 | bytes 10485760 | tf_op jit(solution)/shard_map/dot_general | solution.py:55
  299.3 54.5 %all-to-all-done.3 = bf16[16,128,1024]{2,1,0:T(8,128)(2,1)} async-done(((bf16[16,128,1024]{2,1,0:T(8,128)(2,1)}), bf16[16,128,1024]{2,1,0:T(8,128)(2,1)}, u32[]{:S(2)}, u32[]{:S(2)}) %all-to-all-start.3) | async-done | bytes 4194336 | tf_op jit(solution)/shard_map/all_to_all | solution.py:29
  353.8 12.5 %convolution_convert_fusion = bf16[768,2048]{1,0:T(8,128)(2,1)} fusion(bf16[2048,1024]{1,0:T(8,128)(2,1)} %bitcast.26, f32[768,1024]{1,0:T(8,128)} %fusion.36, bf16[768,2048]{1,0:T(8,128)(2,1)} %all-gather.3.cloned.1.call-done, bf16[2048,1024]{1,0:T(8,128)(2,1)} %bitcast.124), kind=kOutput, calls=%fused_computation.5 | convolution fusion | flops 6448742400 | bytes 17825792 | tf_op jit(solution)/shard_map/rf,df->rd/dot_general | solution.py:58
  366.3 0.0 reduce-scatter.2.cloned.1.call-update
  366.3 0.0 all-gather.5.cloned.1.call-start
  366.4 24.9 %reduce-scatter.2.cloned.1.call-done = bf16[768,1024]{1,0:T(8,128)(2,1)} async-done(((bf16[768,2048]{1,0:T(8,128)(2,1)}), bf16[768,1024]{1,0:T(8,128)(2,1)}) %reduce-scatter.2.cloned.1.call-update) | async-done | bytes 1572880 | tf_op jit(solution)/shard_map/reduce_scatter | solution.py:59
  391.3 44.9 %all_to_all.40 = bf16[16,48,1024]{2,1,0:T(8,128)(2,1)} all-to-all(bf16[16,48,1024]{2,1,0:T(8,128)(2,1)} %bitcast.129), channel_id=1, replica_groups=mesh['fs'=16,'tp'=2] {'fs'}, dimensions={0} | all-to-all | bytes 3145728 | tf_op jit(solution)/shard_map/all_to_all | solution.py:62
  436.2 0.0 all-gather.5.cloned.1.call-update
  436.2 10.6 %all-gather.5.cloned.1.call-done = bf16[16,48,2048]{2,1,0:T(8,128)(2,1)} async-done(((bf16[16,48,1024]{2,1,0:T(8,128)(2,1)}), bf16[16,48,2048]{2,1,0:T(8,128)(2,1)}) %all-gather.5.cloned.1.call-update) | async-done | bytes 3145744 | tf_op jit(solution)/shard_map/all_gather | solution.py:65
  446.8 7.3 %gather_fusion.1 = bf16[384,2048]{1,0:T(8,128)(2,1)} fusion(bf16[768,2048]{1,0:T(8,128)(2,1)} %bitcast.107, s32[1024]{0:T(1024)S(1)} %pad_clamp_fusion), kind=kCustom, calls=%fused_computation.1 | custom fusion | bytes 3147264 | tf_op jit(solution)/shard_map/gather | solution.py:66
  454.1 3.4 reshape.183
  457.5 2.4 fusion.35
  460.0 2.5 fusion.6
  462.4 4.8 %copy.85 = bf16[1,2048,1024]{2,1,0:T(8,128)(2,1)} copy(bf16[1,2048,1024]{2,1,0:T(8,128)(2,1)} %bitcast.32) | data formatting | bytes 8388608
  467.3 2.0 copy.86
  469.3 4.6 copy.87
  (15 shorter events, 0.1 us)
Async XLA Ops:
  22.2 11.1 %copy-start.2 = (f32[128]{0:T(128)S(1)}, f32[128]{0:T(128)}, u32[]{:S(2)}) copy-start(f32[128]{0:T(128)} %param.10) | copy-start | bytes 1540
  24.9 42.6 %all-to-all-start = ((bf16[16,48,1024]{2,1,0:T(8,128)(2,1)}), bf16[16,48,1024]{2,1,0:T(8,128)(2,1)}, u32[]{:S(2)}, u32[]{:S(2)}) async-start(bf16[16,48,1024]{2,1,0:T(8,128)(2,1)} %constant_dynamic-slice_fusion), calls=%async_computation | async-start | bytes 3145728 | tf_op jit(solution)/shard_map/all_to_all | solution.py:51
  171.2 83.0 %all-to-all-start.1 = ((bf16[16,128,1024]{2,1,0:T(8,128)(2,1)}), bf16[16,128,1024]{2,1,0:T(8,128)(2,1)}, u32[]{:S(2)}, u32[]{:S(2)}) async-start(bf16[16,128,1024]{2,1,0:T(8,128)(2,1)} %bitcast.127), calls=%async_computation.1 | async-start | bytes 8388608 | tf_op jit(solution)/shard_map/all_to_all | solution.py:27
  256.8 97.0 %all-to-all-start.3 = ((bf16[16,128,1024]{2,1,0:T(8,128)(2,1)}), bf16[16,128,1024]{2,1,0:T(8,128)(2,1)}, u32[]{:S(2)}, u32[]{:S(2)}) async-start(bf16[16,128,1024]{2,1,0:T(8,128)(2,1)} %bitcast.126), calls=%async_computation.3 | async-start | bytes 8388608 | tf_op jit(solution)/shard_map/all_to_all | solution.py:29
  275.3 15.7 %all-gather.3.cloned.1.call-start = ((), (), s32[]{:S(2)}) async-start(), calls=%async_computation.6 | async-start | bytes 4718592 | tf_op jit(solution)/shard_map/all_gather | solution.py:54
  276.1 115.2 %reduce-scatter.2.cloned.1.call-start = ((), (), s32[]{:S(2)}) async-start(), calls=%async_computation.7 | async-start | bytes 4718592 | tf_op jit(solution)/shard_map/reduce_scatter | solution.py:59
  366.3 69.9 %copy-start.1 = (f32[192,2]{0,1:T(2,128)S(1)}, f32[192,2]{0,1:T(2,128)}, u32[]{:S(2)}) copy-start(f32[192,2]{0,1:T(2,128)} %param.9) | copy-start | bytes 4612
  366.3 80.4 %all-gather.5.cloned.1.call-start = ((), (), s32[]{:S(2)}) async-start(), calls=%async_computation.8 | async-start | bytes 4718592 | tf_op jit(solution)/shard_map/all_gather | solution.py:65
  462.4 4.8 %copy-start = (bf16[16,1,128,1024]{3,2,1,0:T(8,128)(2,1)S(1)}, bf16[16,1,128,1024]{3,2,1,0:T(8,128)(2,1)}, u32[]{:S(2)}) copy-start(bf16[16,1,128,1024]{3,2,1,0:T(8,128)(2,1)} %all_to_all.39) | copy-start | bytes 12582916
Sparse Core Ops, SparseCore 0:
  277.7 13.3 all-gather.2
  366.5 24.7 reduce-scatter.1
  436.3 10.4 all-gather.4
